TPU v7x, 128 devices: a whole 4x4x4 slice. The times are simulated.
128 devices in a mesh: sp: 64 (over z, y, x), tp: 2 (over core).
Axes of the slice: x: 4, y: 4, z: 4, core: 2. Of those that a mesh axis runs over, the one named last changes fastest.
Arguments:
- residual: bfloat16 [16384, 2048], P(('sp', 'tp')), may hold values from -6 to 6
- query_nope: bfloat16 [16384, 1024], P('sp', 'tp'), may hold values from -24 to 24
- query_rope: bfloat16 [16384, 512], P('sp', 'tp'), may hold values from -400 to 400
- latent: bfloat16 [16384, 256], P(('sp', 'tp')), may hold values from -6 to 6
- key_rope: bfloat16 [16384, 64], P(('sp', 'tp')), may hold values from -6 to 6
- key_up: bfloat16 [256, 1024], P(None, 'tp'), may hold values from -0.375 to 0.375
- value_up: bfloat16 [256, 1024], P(None, 'tp'), may hold values from -0.375 to 0.375
- out_proj: bfloat16 [1024, 2048], replicated, may hold values from -0.375 to 0.375
- norm_gain: float32 [2048], replicated, may hold values from 0.1 to 1.9
- routes: int32 [16384, 2], P(('sp', 'tp')), may hold values from 0 to 63, all different within a row; in each aligned block of 128 rows (0 to 127, 128 to 255, ...) at most 8 rows name the same one
- route_weight: float32 [16384, 2], P(('sp', 'tp')), may hold values from 0.3 to 2.5
- w_gate: bfloat16 [64, 2048, 512], P('sp', None, 'tp'), may hold values from -0.125 to 0.125
- w_up: bfloat16 [64, 2048, 512], P('sp', None, 'tp'), may hold values from -0.125 to 0.125
- w_down: bfloat16 [64, 512, 2048], P('sp', 'tp'), may hold values from -0.25 to 0.25
Outputs:
- mixed: bfloat16 [16384, 2048], P(('sp', 'tp'))
Inputs may be any that keep to these rules, and one draw needn't show every extreme that they name: `routes`: each row names 2 different experts. Among the rows of one device no expert is named more than 8 times, a bound that some block reaches by the rows of some device.
All inputs are finite; a program needn't handle non-finite values.
Results may differ from a plain program's by a relative error of at most 0.015.
Values may be sent and summed in bfloat16 or wider, within the bound.
A program may use at most 128 MiB of HBM per device.

v0:
```python
import jax
import jax.numpy as jnp
from jax import lax
from jax.sharding import PartitionSpec as P

QK_NOPE = 128
QK_ROPE = 64
V_DIM = 128
SEGMENT = 64


EPSILON = 1e-06
ROPE_BASE = 10000.0
NEG_LARGE = -1e30


def side_by_side(arrays, axis, dim, along):
    both = jnp.concatenate(arrays, axis=along)
    whole, at, finished = (lax.all_gather(both, axis, axis=dim, tiled=True), 0, [])
    for a in arrays:
        finished.append(lax.slice_in_dim(whole, at, at + a.shape[along], axis=along))
        at += a.shape[along]
    return tuple(finished)


def copy_for_each(value, axis):
    copies = jnp.broadcast_to(value, (lax.axis_size(axis), *value.shape))
    return lax.all_to_all(copies, axis, split_axis=0, concat_axis=0, tiled=True)


def laid_out(blocks, dim):
    dims = list(blocks.shape[1:])
    dims[dim] *= blocks.shape[0]
    return jnp.moveaxis(blocks, 0, dim).reshape(dims)


def collect(value, axis, dim):
    blocks = copy_for_each(value, axis)
    return laid_out(blocks, dim)


def split_up(value, dim, count):
    dims = value.shape
    blocks = value.reshape(*dims[:dim], count, dims[dim] // count, *dims[dim + 1 :])
    return jnp.moveaxis(blocks, dim, 0)


def sent_and_summed(value, axis, dim):
    blocks = split_up(value, dim, lax.axis_size(axis))
    arrived = lax.all_to_all(blocks, axis, split_axis=0, concat_axis=0, tiled=True)
    return arrived.astype(jnp.float32).sum(axis=0)


def rotary(values, positions):
    half_width = values.shape[-1] // 2
    inverse = ROPE_BASE ** (-2.0 * jnp.arange(half_width, dtype=jnp.float32) / values.shape[-1])
    angles = positions.astype(jnp.float32)[:, None] * inverse[None, :]
    cosine = jnp.cos(angles)
    sine_part = jnp.sin(angles)
    if values.ndim == 3:
        cosine = cosine[:, None, :]
        sine_part = sine_part[:, None, :]
    first_half = values[..., :half_width]
    second = values[..., half_width:]
    return jnp.concatenate(
        [first_half * cosine - second * sine_part, second * cosine + first_half * sine_part],
        axis=-1,
    )


def local(
    residual,
    query_nope,
    query_rope,
    latent,
    key_rope,
    key_up,
    value_up,
    out_proj,
    norm_gain,
    routes,
    route_weight,
    w_gate,
    w_up,
    w_down,
):
    tp_count = lax.axis_size("tp")
    tp_index = lax.axis_index("tp")
    sp_index = lax.axis_index("sp")
    row_count = residual.shape[0]
    tok_dev = query_nope.shape[0]
    heads_here = query_nope.shape[1] // QK_NOPE
    score_scale = (QK_NOPE + QK_ROPE) ** (-0.5)
    query_first = sp_index * tok_dev
    query_pos = query_first + jnp.arange(tok_dev, dtype=jnp.int32)
    query_rot = rotary(
        query_rope.astype(jnp.float32).reshape(tok_dev, heads_here, QK_ROPE), query_pos
    ).astype(jnp.bfloat16)
    query_heads = query_nope.reshape(tok_dev, heads_here, QK_NOPE)
    key_pos = query_first + tp_index * row_count + jnp.arange(row_count, dtype=jnp.int32)
    key_rot = rotary(key_rope.astype(jnp.float32), key_pos).astype(jnp.bfloat16)
    query_segment = query_pos // SEGMENT
    last_segment = (query_first + tok_dev - 1) // SEGMENT
    initial = (
        jnp.full((heads_here, tok_dev), NEG_LARGE, jnp.float32),
        jnp.zeros((heads_here, tok_dev), jnp.float32),
        jnp.zeros((tok_dev, heads_here, V_DIM), jnp.float32),
    )
    lat_rows, rot_rows = side_by_side((latent, key_rot), ("sp", "tp"), 0, 1)
    piece_rows = lat_rows.shape[0]
    key_block = piece_rows
    while key_block > 2048 and key_block % 2 == 0:
        key_block //= 2
    block_count = piece_rows // key_block

    def one_block(state_now, inputs):
        lat_block, rot_block, offset = inputs
        key_nope = jnp.dot(lat_block, key_up, preferred_element_type=jnp.float32).astype(
            jnp.bfloat16
        )
        key_nope = key_nope.reshape(key_block, heads_here, QK_NOPE)
        value_rows = jnp.dot(lat_block, value_up, preferred_element_type=jnp.float32).astype(
            jnp.bfloat16
        )
        value_rows = value_rows.reshape(key_block, heads_here, V_DIM)
        scores = jnp.einsum(
            "qhd,khd->hqk", query_heads, key_nope, preferred_element_type=jnp.float32
        )
        scores = (
            scores
            + jnp.einsum("qhr,kr->hqk", query_rot, rot_block, preferred_element_type=jnp.float32)
        ) * score_scale
        key_segment = (offset + jnp.arange(key_block, dtype=jnp.int32)) // SEGMENT
        allowed = (key_segment[None, :] <= query_segment[:, None])[None]
        scores = jnp.where(allowed, scores, NEG_LARGE)
        old_max, old_sum, old_acc = state_now
        new_max = jnp.maximum(old_max, jnp.max(scores, axis=-1))
        weights = jnp.where(allowed, jnp.exp(scores - new_max[:, :, None]), 0.0)
        shrink = jnp.exp(old_max - new_max)
        new_sum = old_sum * shrink + jnp.sum(weights, axis=-1)
        new_acc = old_acc * shrink.T[:, :, None] + jnp.einsum(
            "hqk,khv->qhv",
            weights.astype(jnp.bfloat16),
            value_rows,
            preferred_element_type=jnp.float32,
        )
        return ((new_max, new_sum, new_acc), None)

    def compute(state_now):
        result, unused = lax.scan(
            one_block,
            state_now,
            (
                lat_rows.reshape(block_count, key_block, lat_rows.shape[1]),
                rot_rows.reshape(block_count, key_block, rot_rows.shape[1]),
                jnp.arange(block_count, dtype=jnp.int32) * key_block,
            ),
        )
        return result

    def keep_state(state_now):
        return state_now

    row_max, weight_sum, weighted = lax.cond(
        jnp.int32(0) // SEGMENT <= last_segment, compute, keep_state, initial
    )
    attn_out = (
        (weighted / weight_sum.T[:, :, None])
        .astype(jnp.bfloat16)
        .reshape(tok_dev, heads_here * V_DIM)
    )
    all_heads = lax.all_to_all(attn_out, "tp", split_axis=0, concat_axis=1, tiled=True)
    projected = jnp.dot(all_heads, out_proj, preferred_element_type=jnp.float32)
    hidden_wide = residual.astype(jnp.float32) + projected
    hidden = hidden_wide.astype(jnp.bfloat16)
    hidden_wide = hidden.astype(jnp.float32)
    normed = hidden_wide * lax.rsqrt(
        jnp.mean(hidden_wide * hidden_wide, axis=-1, keepdims=True) + EPSILON
    )
    normed = (normed * norm_gain[None, :]).astype(jnp.bfloat16)
    expert_count = lax.axis_size("sp")
    capacity = max(2, 2 * (row_count * tp_count) // expert_count)
    top_count = routes.shape[1]
    width = normed.shape[1]
    flat_expert = routes.reshape(-1)
    onehot = (flat_expert[:, None] == jnp.arange(expert_count, dtype=jnp.int32)[None, :]).astype(
        jnp.int32
    )
    slot_rank = jnp.sum(jnp.cumsum(onehot, axis=0) * onehot, axis=1) - 1
    slot_index = flat_expert * capacity + slot_rank
    outgoing = (
        jnp.zeros((expert_count * capacity, width), jnp.bfloat16)
        .at[slot_index]
        .set(jnp.repeat(normed, top_count, axis=0))
    )
    gate_weight = w_gate[0]
    up_weight = w_up[0]
    down_weight = w_down[0]
    shard_piece = collect(
        lax.all_to_all(
            outgoing.reshape(expert_count, capacity, width),
            "sp",
            split_axis=0,
            concat_axis=0,
            tiled=True,
        ),
        "tp",
        0,
    )
    gate_part = jnp.dot(shard_piece, gate_weight, preferred_element_type=jnp.float32)
    up_part = jnp.dot(shard_piece, up_weight, preferred_element_type=jnp.float32)
    activated = (jax.nn.silu(gate_part) * up_part).astype(jnp.bfloat16)
    product = jnp.dot(activated, down_weight, preferred_element_type=jnp.float32)
    summed = sent_and_summed(
        lax.optimization_barrier(product.astype(jnp.bfloat16))
        .astype(jnp.float32)
        .astype(jnp.bfloat16),
        "tp",
        0,
    )
    returned = summed.astype(jnp.bfloat16)
    back_rows = lax.all_to_all(returned, "sp", split_axis=0, concat_axis=0, tiled=True)
    picked = back_rows.reshape(expert_count * capacity, width)[slot_index]
    combined = jnp.sum(
        picked.astype(jnp.float32).reshape(row_count, top_count, width) * route_weight[:, :, None],
        axis=1,
    )
    return (hidden_wide + combined).astype(jnp.bfloat16)


def solution(mesh):
    return jax.shard_map(
        local,
        mesh=mesh,
        in_specs=(
            P(("sp", "tp"), None),
            P("sp", "tp"),
            P("sp", "tp"),
            P(("sp", "tp"), None),
            P(("sp", "tp"), None),
            P(None, "tp"),
            P(None, "tp"),
            P(),
            P(),
            P(("sp", "tp"), None),
            P(("sp", "tp"), None),
            P("sp", None, "tp"),
            P("sp", None, "tp"),
            P("sp", "tp", None),
        ),
        out_specs=P(("sp", "tp"), None),
        check_vma=False,
    )
```

profile of v0, /device:TPU:1, one launch (start us, length us, event | category | flops | bytes accessed | tf_op | source)
XLA Modules:
  0.0 444.2 jit_solution(9489817846854970023)
XLA Ops:
  13.5 84.0 %all-gather.2.cloned.1.call-done = bf16[16384,320]{0,1:T(8,128)(2,1)} async-done(((bf16[128,320]{0,1:T(8,128)(2,1)}), bf16[16384,320]{0,1:T(8,128)(2,1)}) %all-gather.2.cloned.1.call-update) | async-done | bytes 10485776 | tf_op jit(solution)/shard_map/all_gather | solution.py:19
  97.4 201.9 %conditional.1 = (f32[4,256]{1,0:T(4,128)}, f32[256,4,128]{0,2,1:T(8,128)}) conditional(s32[]{:T(128)} %convert_element_type.82, () %tuple.28, (bf16[16384,320]{0,1:T(8,128)(2,1)}, bf16[256,512]{1,0:T(8,128)(2,1)}, s32[256]{0:T(256)S(1)}, s32[256]{0:T(256)S(1)}, s32[]{:T(128)}, /*index=5*/bf16[256,512]{1,0:T(8,128)(2,1)}, ...), branch_computations={%region_0.1_spmd, %region_1.6_spmd.clone} | conditional | flops 2439948032 | bytes 128145352 | solution.py:164
  97.4 7.7 %slice.34 = bf16[16384,256]{0,1:T(8,128)(2,1)} slice(bf16[16384,320]{0,1:T(8,128)(2,1)} %get-tuple-element.261), slice={[0:16384], [0:256]} | slice | bytes 16777216 | tf_op jit(solution)/shard_map/slice | solution.py:21
  105.1 11.9 %copy.78 = bf16[16384,256]{1,0:T(8,128)(2,1)} copy(bf16[16384,256]{0,1:T(8,128)(2,1)} %slice.34) | data formatting | bytes 16777216 | tf_op jit(solution)/shard_map/slice | solution.py:21
  120.7 178.7 %while.20 = (s32[]{:T(128)}, f32[4,256]{1,0:T(4,128)S(1)}, f32[4,256]{1,0:T(4,128)}, f32[256,4,128]{0,2,1:T(8,128)}, s32[8]{0:T(128)S(1)}, /*index=5*/s32[256]{0...) while((s32[]{:T(128)}, f32[4,256]{1,0:T(4,128)S(1)}, ...), condition=%wide.region_5.5_spmd.clone, body=%wide.region_2.4_spmd.clone.sunk | while | flops 2439944192 | bytes 82004680 | solution.py:150
  120.7 2.0 convolution_convert_fusion.5
  125.6 6.5 %fusion.96 = (f32[4,256]{1,0:T(4,128)S(1)}, f32[4,256,2048]{1,2,0:T(8,128)}) fusion(bf16[256,4,64]{0,2,1:T(8,128)(2,1)S(1)} %get-tuple-element.552, bf16[8,2048,64]{1,2,0:T(8,128)(2,1)} %get-tuple-element.551, s32[]{:T(128)} %get-tuple-element.528, f32[4,2048,256]{2,1,0:T(8,128)S(1)} %fusion.95, pred[256,2048]{0,1:T(8,128)(4,1)S(1)} %broadcast_compare_fusion.2), kind=kOutput, calls=%fused_computation.105.clone.1 | convolution fusion | flops 276823040 | bytes 17699328 | tf_op jit(solution)/shard_map/cond/branch_1_fun/while/body/eval_jaxpr/qhr,kr->hqk/dot_general | solution.py:131
  132.1 2.1 convolution_convert_fusion.6
  134.3 6.0 %fusion.100 = f32[256,4,128]{0,2,1:T(8,128)} fusion(bf16[2048,4,128]{0,2,1:T(8,128)(2,1)S(1)} %bitcast.116, f32[4,256,2048]{1,2,0:T(8,128)} %get-tuple-element.512, f32[4,256]{1,0:T(4,128)S(1)} %get-tuple-element.543, pred[256,2048]{0,1:T(8,128)(4,1)S(1)} %broadcast_compare_fusion.2, f32[256,4,128]{0,2,1:T(8,128)} %get-tuple-element.531, ...), kind=kOutput, calls=%fused_computation.15.clone.1 | convolution fusion | flops 543555584 | bytes 12066817 | tf_op jit(solution)/shard_map/cond/branch_1_fun/while/body/eval_jaxpr/hqk,khv->qhv/dot_general | solution.py:141
  142.4 2.0 convolution_convert_fusion.5
  147.3 6.5 %fusion.96 = (f32[4,256]{1,0:T(4,128)S(1)}, f32[4,256,2048]{1,2,0:T(8,128)}) fusion(bf16[256,4,64]{0,2,1:T(8,128)(2,1)S(1)} %get-tuple-element.552, bf16[8,2048,64]{1,2,0:T(8,128)(2,1)} %get-tuple-element.551, s32[]{:T(128)} %get-tuple-element.528, f32[4,2048,256]{2,1,0:T(8,128)S(1)} %fusion.95, pred[256,2048]{0,1:T(8,128)(4,1)S(1)} %broadcast_compare_fusion.2), kind=kOutput, calls=%fused_computation.105.clone.1 | convolution fusion | flops 276823040 | bytes 17699328 | tf_op jit(solution)/shard_map/cond/branch_1_fun/while/body/eval_jaxpr/qhr,kr->hqk/dot_general | solution.py:131
  153.8 2.1 convolution_convert_fusion.6
  156.0 6.1 %fusion.100 = f32[256,4,128]{0,2,1:T(8,128)} fusion(bf16[2048,4,128]{0,2,1:T(8,128)(2,1)S(1)} %bitcast.116, f32[4,256,2048]{1,2,0:T(8,128)} %get-tuple-element.512, f32[4,256]{1,0:T(4,128)S(1)} %get-tuple-element.543, pred[256,2048]{0,1:T(8,128)(4,1)S(1)} %broadcast_compare_fusion.2, f32[256,4,128]{0,2,1:T(8,128)} %get-tuple-element.531, ...), kind=kOutput, calls=%fused_computation.15.clone.1 | convolution fusion | flops 543555584 | bytes 12066817 | tf_op jit(solution)/shard_map/cond/branch_1_fun/while/body/eval_jaxpr/hqk,khv->qhv/dot_general | solution.py:141
  164.8 2.0 convolution_convert_fusion.5
  169.7 6.5 %fusion.96 = (f32[4,256]{1,0:T(4,128)S(1)}, f32[4,256,2048]{1,2,0:T(8,128)}) fusion(bf16[256,4,64]{0,2,1:T(8,128)(2,1)S(1)} %get-tuple-element.552, bf16[8,2048,64]{1,2,0:T(8,128)(2,1)} %get-tuple-element.551, s32[]{:T(128)} %get-tuple-element.528, f32[4,2048,256]{2,1,0:T(8,128)S(1)} %fusion.95, pred[256,2048]{0,1:T(8,128)(4,1)S(1)} %broadcast_compare_fusion.2), kind=kOutput, calls=%fused_computation.105.clone.1 | convolution fusion | flops 276823040 | bytes 17699328 | tf_op jit(solution)/shard_map/cond/branch_1_fun/while/body/eval_jaxpr/qhr,kr->hqk/dot_general | solution.py:131
  176.2 2.1 convolution_convert_fusion.6
  178.4 6.1 %fusion.100 = f32[256,4,128]{0,2,1:T(8,128)} fusion(bf16[2048,4,128]{0,2,1:T(8,128)(2,1)S(1)} %bitcast.116, f32[4,256,2048]{1,2,0:T(8,128)} %get-tuple-element.512, f32[4,256]{1,0:T(4,128)S(1)} %get-tuple-element.543, pred[256,2048]{0,1:T(8,128)(4,1)S(1)} %broadcast_compare_fusion.2, f32[256,4,128]{0,2,1:T(8,128)} %get-tuple-element.531, ...), kind=kOutput, calls=%fused_computation.15.clone.1 | convolution fusion | flops 543555584 | bytes 12066817 | tf_op jit(solution)/shard_map/cond/branch_1_fun/while/body/eval_jaxpr/hqk,khv->qhv/dot_general | solution.py:141
  192.1 6.5 %fusion.96 = (f32[4,256]{1,0:T(4,128)S(1)}, f32[4,256,2048]{1,2,0:T(8,128)}) fusion(bf16[256,4,64]{0,2,1:T(8,128)(2,1)S(1)} %get-tuple-element.552, bf16[8,2048,64]{1,2,0:T(8,128)(2,1)} %get-tuple-element.551, s32[]{:T(128)} %get-tuple-element.528, f32[4,2048,256]{2,1,0:T(8,128)S(1)} %fusion.95, pred[256,2048]{0,1:T(8,128)(4,1)S(1)} %broadcast_compare_fusion.2), kind=kOutput, calls=%fused_computation.105.clone.1 | convolution fusion | flops 276823040 | bytes 17699328 | tf_op jit(solution)/shard_map/cond/branch_1_fun/while/body/eval_jaxpr/qhr,kr->hqk/dot_general | solution.py:131
  198.7 2.1 convolution_convert_fusion.6
  200.8 6.1 %fusion.100 = f32[256,4,128]{0,2,1:T(8,128)} fusion(bf16[2048,4,128]{0,2,1:T(8,128)(2,1)S(1)} %bitcast.116, f32[4,256,2048]{1,2,0:T(8,128)} %get-tuple-element.512, f32[4,256]{1,0:T(4,128)S(1)} %get-tuple-element.543, pred[256,2048]{0,1:T(8,128)(4,1)S(1)} %broadcast_compare_fusion.2, f32[256,4,128]{0,2,1:T(8,128)} %get-tuple-element.531, ...), kind=kOutput, calls=%fused_computation.15.clone.1 | convolution fusion | flops 543555584 | bytes 12066817 | tf_op jit(solution)/shard_map/cond/branch_1_fun/while/body/eval_jaxpr/hqk,khv->qhv/dot_general | solution.py:141
  214.6 6.5 %fusion.96 = (f32[4,256]{1,0:T(4,128)S(1)}, f32[4,256,2048]{1,2,0:T(8,128)}) fusion(bf16[256,4,64]{0,2,1:T(8,128)(2,1)S(1)} %get-tuple-element.552, bf16[8,2048,64]{1,2,0:T(8,128)(2,1)} %get-tuple-element.551, s32[]{:T(128)} %get-tuple-element.528, f32[4,2048,256]{2,1,0:T(8,128)S(1)} %fusion.95, pred[256,2048]{0,1:T(8,128)(4,1)S(1)} %broadcast_compare_fusion.2), kind=kOutput, calls=%fused_computation.105.clone.1 | convolution fusion | flops 276823040 | bytes 17699328 | tf_op jit(solution)/shard_map/cond/branch_1_fun/while/body/eval_jaxpr/qhr,kr->hqk/dot_general | solution.py:131
  221.1 2.1 convolution_convert_fusion.6
  223.2 6.1 %fusion.100 = f32[256,4,128]{0,2,1:T(8,128)} fusion(bf16[2048,4,128]{0,2,1:T(8,128)(2,1)S(1)} %bitcast.116, f32[4,256,2048]{1,2,0:T(8,128)} %get-tuple-element.512, f32[4,256]{1,0:T(4,128)S(1)} %get-tuple-element.543, pred[256,2048]{0,1:T(8,128)(4,1)S(1)} %broadcast_compare_fusion.2, f32[256,4,128]{0,2,1:T(8,128)} %get-tuple-element.531, ...), kind=kOutput, calls=%fused_computation.15.clone.1 | convolution fusion | flops 543555584 | bytes 12066817 | tf_op jit(solution)/shard_map/cond/branch_1_fun/while/body/eval_jaxpr/hqk,khv->qhv/dot_general | solution.py:141
  237.0 6.5 %fusion.96 = (f32[4,256]{1,0:T(4,128)S(1)}, f32[4,256,2048]{1,2,0:T(8,128)}) fusion(bf16[256,4,64]{0,2,1:T(8,128)(2,1)S(1)} %get-tuple-element.552, bf16[8,2048,64]{1,2,0:T(8,128)(2,1)} %get-tuple-element.551, s32[]{:T(128)} %get-tuple-element.528, f32[4,2048,256]{2,1,0:T(8,128)S(1)} %fusion.95, pred[256,2048]{0,1:T(8,128)(4,1)S(1)} %broadcast_compare_fusion.2), kind=kOutput, calls=%fused_computation.105.clone.1 | convolution fusion | flops 276823040 | bytes 17699328 | tf_op jit(solution)/shard_map/cond/branch_1_fun/while/body/eval_jaxpr/qhr,kr->hqk/dot_general | solution.py:131
  243.5 2.1 convolution_convert_fusion.6
  245.7 6.1 %fusion.100 = f32[256,4,128]{0,2,1:T(8,128)} fusion(bf16[2048,4,128]{0,2,1:T(8,128)(2,1)S(1)} %bitcast.116, f32[4,256,2048]{1,2,0:T(8,128)} %get-tuple-element.512, f32[4,256]{1,0:T(4,128)S(1)} %get-tuple-element.543, pred[256,2048]{0,1:T(8,128)(4,1)S(1)} %broadcast_compare_fusion.2, f32[256,4,128]{0,2,1:T(8,128)} %get-tuple-element.531, ...), kind=kOutput, calls=%fused_computation.15.clone.1 | convolution fusion | flops 543555584 | bytes 12066817 | tf_op jit(solution)/shard_map/cond/branch_1_fun/while/body/eval_jaxpr/hqk,khv->qhv/dot_general | solution.py:141
  259.4 6.5 %fusion.96 = (f32[4,256]{1,0:T(4,128)S(1)}, f32[4,256,2048]{1,2,0:T(8,128)}) fusion(bf16[256,4,64]{0,2,1:T(8,128)(2,1)S(1)} %get-tuple-element.552, bf16[8,2048,64]{1,2,0:T(8,128)(2,1)} %get-tuple-element.551, s32[]{:T(128)} %get-tuple-element.528, f32[4,2048,256]{2,1,0:T(8,128)S(1)} %fusion.95, pred[256,2048]{0,1:T(8,128)(4,1)S(1)} %broadcast_compare_fusion.2), kind=kOutput, calls=%fused_computation.105.clone.1 | convolution fusion | flops 276823040 | bytes 17699328 | tf_op jit(solution)/shard_map/cond/branch_1_fun/while/body/eval_jaxpr/qhr,kr->hqk/dot_general | solution.py:131
  265.9 2.1 convolution_convert_fusion.6
  268.1 6.1 %fusion.100 = f32[256,4,128]{0,2,1:T(8,128)} fusion(bf16[2048,4,128]{0,2,1:T(8,128)(2,1)S(1)} %bitcast.116, f32[4,256,2048]{1,2,0:T(8,128)} %get-tuple-element.512, f32[4,256]{1,0:T(4,128)S(1)} %get-tuple-element.543, pred[256,2048]{0,1:T(8,128)(4,1)S(1)} %broadcast_compare_fusion.2, f32[256,4,128]{0,2,1:T(8,128)} %get-tuple-element.531, ...), kind=kOutput, calls=%fused_computation.15.clone.1 | convolution fusion | flops 543555584 | bytes 12066817 | tf_op jit(solution)/shard_map/cond/branch_1_fun/while/body/eval_jaxpr/hqk,khv->qhv/dot_general | solution.py:141
  277.0 2.0 convolution_convert_fusion.5
  281.8 6.5 %fusion.96 = (f32[4,256]{1,0:T(4,128)S(1)}, f32[4,256,2048]{1,2,0:T(8,128)}) fusion(bf16[256,4,64]{0,2,1:T(8,128)(2,1)S(1)} %get-tuple-element.552, bf16[8,2048,64]{1,2,0:T(8,128)(2,1)} %get-tuple-element.551, s32[]{:T(128)} %get-tuple-element.528, f32[4,2048,256]{2,1,0:T(8,128)S(1)} %fusion.95, pred[256,2048]{0,1:T(8,128)(4,1)S(1)} %broadcast_compare_fusion.2), kind=kOutput, calls=%fused_computation.105.clone.1 | convolution fusion | flops 276823040 | bytes 17699328 | tf_op jit(solution)/shard_map/cond/branch_1_fun/while/body/eval_jaxpr/qhr,kr->hqk/dot_general | solution.py:131
  288.4 2.1 convolution_convert_fusion.6
  290.5 6.1 %fusion.100 = f32[256,4,128]{0,2,1:T(8,128)} fusion(bf16[2048,4,128]{0,2,1:T(8,128)(2,1)S(1)} %bitcast.116, f32[4,256,2048]{1,2,0:T(8,128)} %get-tuple-element.512, f32[4,256]{1,0:T(4,128)S(1)} %get-tuple-element.543, pred[256,2048]{0,1:T(8,128)(4,1)S(1)} %broadcast_compare_fusion.2, f32[256,4,128]{0,2,1:T(8,128)} %get-tuple-element.531, ...), kind=kOutput, calls=%fused_computation.15.clone.1 | convolution fusion | flops 543555584 | bytes 12066817 | tf_op jit(solution)/shard_map/cond/branch_1_fun/while/body/eval_jaxpr/hqk,khv->qhv/dot_general | solution.py:141
  300.7 3.9 all_to_all.39
  304.8 3.0 multiply_reduce_fusion.1
  310.9 3.5 scatter_custom_fusion
  314.4 37.3 %all_to_all.40 = bf16[64,8,2048]{2,1,0:T(8,128)(2,1)S(1)} all-to-all(bf16[64,8,2048]{2,1,0:T(8,128)(2,1)S(1)} %bitcast.118), channel_id=1, replica_groups=mesh['sp'=64,'tp'=2] {'sp'}, dimensions={0} | all-to-all | bytes 4194304 | tf_op jit(solution)/shard_map/all_to_all | solution.py:200
  353.4 8.7 %all_to_all.41 = bf16[2,64,8,2048]{3,1,2,0:T(8,128)(2,1)S(1)} all-to-all(bf16[2,64,8,2048]{3,1,2,0:T(8,128)(2,1)S(1)} %broadcast_in_dim.75), channel_id=1, replica_groups=mesh['sp'=64,'tp'=2] {'tp'}, dimensions={0} | all-to-all | bytes 8388608 | tf_op jit(solution)/shard_map/all_to_all | solution.py:28
  365.9 8.5 %convolution_convert_fusion.2 = bf16[128,8,2048]{2,0,1:T(8,128)(2,1)} fusion(bf16[128,8,2048]{2,0,1:T(8,128)(2,1)} %bitcast.122, bf16[1,256,2048]{2,1,0:T(8,128)(2,1)S(1)} %copy-done, bf16[1,2048,256]{2,1,0:T(8,128)(2,1)S(1)} %copy-done.11, f32[128,8,256]{2,0,1:T(8,128)S(1)} %fusion.36), kind=kOutput, calls=%fused_computation.48 | convolution fusion | flops 2151153664 | bytes 11534336 | tf_op jit(solution)/shard_map/dot_general | solution.py:213
  374.4 2.5 copy.92
  376.9 8.3 %all_to_all.42 = bf16[2,64,8,2048]{3,1,2,0:T(8,128)(2,1)} all-to-all(bf16[2,64,8,2048]{3,1,2,0:T(8,128)(2,1)S(1)} %copy.92), channel_id=1, replica_groups=mesh['sp'=64,'tp'=2] {'tp'}, dimensions={0} | all-to-all | bytes 8388608 | tf_op jit(solution)/shard_map/all_to_all | solution.py:50
  385.2 3.5 reduce_sum.53
  388.7 2.5 copy.94
  391.2 5.4 %all-to-all-start.4 = ((bf16[64,8,2048]{2,1,0:T(8,128)(2,1)}), bf16[64,8,2048]{2,1,0:T(8,128)(2,1)S(1)}, u32[]{:S(2)}, u32[]{:S(2)}) async-start(bf16[64,8,2048]{2,1,0:T(8,128)(2,1)} %copy.94), calls=%async_computation.4 | async-start | bytes 4194304 | tf_op jit(solution)/shard_map/all_to_all | solution.py:222
  396.7 29.0 %all-to-all-done.4 = bf16[64,8,2048]{2,1,0:T(8,128)(2,1)S(1)} async-done(((bf16[64,8,2048]{2,1,0:T(8,128)(2,1)}), bf16[64,8,2048]{2,1,0:T(8,128)(2,1)S(1)}, u32[]{:S(2)}, u32[]{:S(2)}) %all-to-all-start.4) | async-done | bytes 2097184 | tf_op jit(solution)/shard_map/all_to_all | solution.py:222
  425.7 2.3 gather_fusion
  428.1 3.5 reshape.240
  431.5 4.8 %multiply_reduce_fusion = f32[128,2048]{1,0:T(8,128)S(1)} fusion(f32[128,2,2048]{2,1,0:T(2,128)} %reshape.240, f32[128,2]{1,0:T(8,128)S(1)} %copy.95), kind=kLoop, calls=%fused_computation.52 | loop fusion | flops 786432 | bytes 3146752 | tf_op jit(solution)/shard_map/reduce_sum | solution.py:224
  (184 shorter events, 74.2 us)
Async XLA Ops:
  6.5 359.4 %copy-start = (bf16[1,256,2048]{2,1,0:T(8,128)(2,1)S(1)}, bf16[1,256,2048]{2,1,0:T(8,128)(2,1)}, u32[]{:S(2)}) copy-start(bf16[1,256,2048]{2,1,0:T(8,128)(2,1)} %param.31) | copy-start | bytes 3145732
  6.5 90.9 %all-gather.2.cloned.1.call-start = ((), (), s32[]{:S(2)}) async-start(), calls=%async_computation.5 | async-start | bytes 10567680 | tf_op jit(solution)/shard_map/all_gather | solution.py:19
  97.4 207.4 %copy-start.6 = (bf16[128,2048]{1,0:T(8,128)(2,1)S(1)}, bf16[128,2048]{1,0:T(8,128)(2,1)}, u32[]{:S(2)}) copy-start(bf16[128,2048]{1,0:T(8,128)(2,1)} %param.18) | copy-start | bytes 1572868
  117.0 3.3 copy-start.7
  117.0 3.6 copy-start.3
  117.0 3.6 copy-start.4
  132.1 8.2 %slice-start = ((s8[8388608]{0:T(1024)(128)(4,1)}), s8[4194304]{0:T(1024)(128)(4,1)S(1)}, s32[]{:S(2)}) async-start(s8[8388608]{0:T(1024)(128)(4,1)} %bitcast.112), calls=%async_computation.6 | async-start | bytes 8388608 | tf_op jit(solution)/shard_map/cond/branch_1_fun/while
  134.3 6.0 %slice-start.1 = ((s8[8388608]{0:T(1024)(128)(4,1)}), s8[4194304]{0:T(1024)(128)(4,1)S(1)}, s32[]{:S(2)}) async-start(s8[8388608]{0:T(1024)(128)(4,1)} %bitcast.112), calls=%async_computation.7 | async-start | bytes 8388608 | tf_op jit(solution)/shard_map/cond/branch_1_fun/while
  153.8 8.2 %slice-start = ((s8[8388608]{0:T(1024)(128)(4,1)}), s8[4194304]{0:T(1024)(128)(4,1)S(1)}, s32[]{:S(2)}) async-start(s8[8388608]{0:T(1024)(128)(4,1)} %bitcast.112), calls=%async_computation.6 | async-start | bytes 8388608 | tf_op jit(solution)/shard_map/cond/branch_1_fun/while
  156.0 6.1 %slice-start.1 = ((s8[8388608]{0:T(1024)(128)(4,1)}), s8[4194304]{0:T(1024)(128)(4,1)S(1)}, s32[]{:S(2)}) async-start(s8[8388608]{0:T(1024)(128)(4,1)} %bitcast.112), calls=%async_computation.7 | async-start | bytes 8388608 | tf_op jit(solution)/shard_map/cond/branch_1_fun/while
  176.2 8.2 %slice-start = ((s8[8388608]{0:T(1024)(128)(4,1)}), s8[4194304]{0:T(1024)(128)(4,1)S(1)}, s32[]{:S(2)}) async-start(s8[8388608]{0:T(1024)(128)(4,1)} %bitcast.112), calls=%async_computation.6 | async-start | bytes 8388608 | tf_op jit(solution)/shard_map/cond/branch_1_fun/while
  178.4 6.1 %slice-start.1 = ((s8[8388608]{0:T(1024)(128)(4,1)}), s8[4194304]{0:T(1024)(128)(4,1)S(1)}, s32[]{:S(2)}) async-start(s8[8388608]{0:T(1024)(128)(4,1)} %bitcast.112), calls=%async_computation.7 | async-start | bytes 8388608 | tf_op jit(solution)/shard_map/cond/branch_1_fun/while
  198.7 8.2 %slice-start = ((s8[8388608]{0:T(1024)(128)(4,1)}), s8[4194304]{0:T(1024)(128)(4,1)S(1)}, s32[]{:S(2)}) async-start(s8[8388608]{0:T(1024)(128)(4,1)} %bitcast.112), calls=%async_computation.6 | async-start | bytes 8388608 | tf_op jit(solution)/shard_map/cond/branch_1_fun/while
  200.8 6.1 %slice-start.1 = ((s8[8388608]{0:T(1024)(128)(4,1)}), s8[4194304]{0:T(1024)(128)(4,1)S(1)}, s32[]{:S(2)}) async-start(s8[8388608]{0:T(1024)(128)(4,1)} %bitcast.112), calls=%async_computation.7 | async-start | bytes 8388608 | tf_op jit(solution)/shard_map/cond/branch_1_fun/while
  221.1 8.2 %slice-start = ((s8[8388608]{0:T(1024)(128)(4,1)}), s8[4194304]{0:T(1024)(128)(4,1)S(1)}, s32[]{:S(2)}) async-start(s8[8388608]{0:T(1024)(128)(4,1)} %bitcast.112), calls=%async_computation.6 | async-start | bytes 8388608 | tf_op jit(solution)/shard_map/cond/branch_1_fun/while
  223.2 6.1 %slice-start.1 = ((s8[8388608]{0:T(1024)(128)(4,1)}), s8[4194304]{0:T(1024)(128)(4,1)S(1)}, s32[]{:S(2)}) async-start(s8[8388608]{0:T(1024)(128)(4,1)} %bitcast.112), calls=%async_computation.7 | async-start | bytes 8388608 | tf_op jit(solution)/shard_map/cond/branch_1_fun/while
  243.5 8.2 %slice-start = ((s8[8388608]{0:T(1024)(128)(4,1)}), s8[4194304]{0:T(1024)(128)(4,1)S(1)}, s32[]{:S(2)}) async-start(s8[8388608]{0:T(1024)(128)(4,1)} %bitcast.112), calls=%async_computation.6 | async-start | bytes 8388608 | tf_op jit(solution)/shard_map/cond/branch_1_fun/while
  245.7 6.1 %slice-start.1 = ((s8[8388608]{0:T(1024)(128)(4,1)}), s8[4194304]{0:T(1024)(128)(4,1)S(1)}, s32[]{:S(2)}) async-start(s8[8388608]{0:T(1024)(128)(4,1)} %bitcast.112), calls=%async_computation.7 | async-start | bytes 8388608 | tf_op jit(solution)/shard_map/cond/branch_1_fun/while
  265.9 8.2 %slice-start = ((s8[8388608]{0:T(1024)(128)(4,1)}), s8[4194304]{0:T(1024)(128)(4,1)S(1)}, s32[]{:S(2)}) async-start(s8[8388608]{0:T(1024)(128)(4,1)} %bitcast.112), calls=%async_computation.6 | async-start | bytes 8388608 | tf_op jit(solution)/shard_map/cond/branch_1_fun/while
  268.1 6.1 %slice-start.1 = ((s8[8388608]{0:T(1024)(128)(4,1)}), s8[4194304]{0:T(1024)(128)(4,1)S(1)}, s32[]{:S(2)}) async-start(s8[8388608]{0:T(1024)(128)(4,1)} %bitcast.112), calls=%async_computation.7 | async-start | bytes 8388608 | tf_op jit(solution)/shard_map/cond/branch_1_fun/while
  288.4 8.2 %slice-start = ((s8[8388608]{0:T(1024)(128)(4,1)}), s8[4194304]{0:T(1024)(128)(4,1)S(1)}, s32[]{:S(2)}) async-start(s8[8388608]{0:T(1024)(128)(4,1)} %bitcast.112), calls=%async_computation.6 | async-start | bytes 8388608 | tf_op jit(solution)/shard_map/cond/branch_1_fun/while
  290.5 6.1 %slice-start.1 = ((s8[8388608]{0:T(1024)(128)(4,1)}), s8[4194304]{0:T(1024)(128)(4,1)S(1)}, s32[]{:S(2)}) async-start(s8[8388608]{0:T(1024)(128)(4,1)} %bitcast.112), calls=%async_computation.7 | async-start | bytes 8388608 | tf_op jit(solution)/shard_map/cond/branch_1_fun/while
  300.5 8.4 %copy-start.8 = (f32[2048]{0:T(1024)S(1)}, f32[2048]{0:T(1024)}, u32[]{:S(2)}) copy-start(f32[2048]{0:T(1024)} %param.26) | copy-start | bytes 24580
  307.8 1.1 copy-start.1
  362.1 2.5 copy-start.10
  362.7 1.9 copy-start.5
  364.7 1.3 copy-start.11
  388.7 7.9 %copy-start.9 = (f32[128,2]{0,1:T(2,128)S(1)}, f32[128,2]{0,1:T(2,128)}, u32[]{:S(2)}) copy-start(f32[128,2]{0,1:T(2,128)} %param.28) | copy-start | bytes 3076
  391.2 34.5 %all-to-all-start.4 = ((bf16[64,8,2048]{2,1,0:T(8,128)(2,1)}), bf16[64,8,2048]{2,1,0:T(8,128)(2,1)S(1)}, u32[]{:S(2)}, u32[]{:S(2)}) async-start(bf16[64,8,2048]{2,1,0:T(8,128)(2,1)} %copy.94), calls=%async_computation.4 | async-start | bytes 4194304 | tf_op jit(solution)/shard_map/all_to_all | solution.py:222
  428.1 8.3 %copy-start.2 = (f32[128,2048]{1,0:T(8,128)S(1)}, f32[128,2048]{1,0:T(8,128)}, u32[]{:S(2)}) copy-start(f32[128,2048]{1,0:T(8,128)} %copy-done.1) | copy-start | bytes 3145732
Sparse Core Ops, SparseCore 0:
  10.1 87.2 all-gather.1
where the time goes:
time: 447 us; the launch traced here: 444 us
  matrix products  157 us (35%)
  waiting for transfers between devices  113 us (25%)
  blocking collectives  58.2 us (13%)
  local copies, waits for them, and re-layouts  53.1 us (12%)
  other arithmetic  43.7 us (10%)
  between operations  13.7 us (3%)
  starting transfers between devices  5.4 us (1%)
    all_gather x1, waiting for transfers between devices, side_by_side(): lax.all_gather(both, axis, axis=dim, tiled=True)  84 us
    dot_general x8, matrix products, one_block(): jnp.einsum('qhr,kr->hqk', query_rot, rot_block, preferred_element_type=jn...  52.2 us
    dot_general x8, matrix products, one_block(): jnp.einsum('hqk,khv->qhv', weights.astype(jnp.bfloat16), value_rows, pref...  48.4 us
    all_to_all x1, blocking collectives, local(): lax.all_to_all(outgoing.reshape(expert_count, capacity, width), 'sp', spl...  37.3 us
    all_to_all x1, waiting for transfers between devices, local(): lax.all_to_all(returned, 'sp', split_axis=0, concat_axis=0, tiled=True)  29 us
    slice x3, local copies, waits for them, and re-layouts, side_by_side(): lax.slice_in_dim(whole, at, at + a.shape[along], axis=along)  21.4 us
    dot_general x8, matrix products, one_block(): jnp.dot(lat_block, value_up, preferred_element_type=jnp.float32)  17.1 us
    dot_general x8, matrix products, one_block(): jnp.dot(lat_block, key_up, preferred_element_type=jnp.float32)  15.8 us
  transfers between devices with their start and end apart: 2, of which 2 were waited for; matrix products, arithmetic and copies ran while one was open for 1% of the time, Pallas kernels for 0%

commit v1 on v0

v1 whole, which is shorter than its diff:
```python
import functools

import jax
import jax.numpy as jnp
from jax import lax
from jax.experimental import pallas as pl
from jax.experimental.pallas import tpu as pltpu
from jax.sharding import PartitionSpec as P

QK_NOPE = 128
QK_ROPE = 64
V_DIM = 128
SEGMENT = 64
EPSILON = 1e-06
ROPE_BASE = 10000.0
NEG_LARGE = -1e30
LOG2_E = 1.4426950408889634
MESH = pl.DeviceIdType.MESH
VMEM = pl.BlockSpec(memory_space=pltpu.VMEM)
ANY = pl.BlockSpec(memory_space=pl.ANY)
SIDE = 4
CHIPS = SIDE**3
TILES = 20
ORDERS = ((2, 1, 0), (1, 0, 2), (0, 2, 1))
COLOURS = ((0, 7), (7, 7), (14, 6))


def rotary_parts(positions, width):
    half = width // 2
    inverse = ROPE_BASE ** (-2.0 * jnp.arange(half, dtype=jnp.float32) / width)
    angles = positions.astype(jnp.float32)[:, None] * inverse[None, :]
    return jnp.cos(angles), jnp.sin(angles)


def rotary(values, positions):
    half = values.shape[-1] // 2
    cosine, sine = rotary_parts(positions, values.shape[-1])
    if values.ndim == 3:
        cosine, sine = cosine[:, None, :], sine[:, None, :]
    first, second = values[..., :half], values[..., half:]
    return jnp.concatenate([first * cosine - second * sine, second * cosine + first * sine], axis=-1)


def place():
    sp, tp = lax.axis_index("sp"), lax.axis_index("tp")
    return sp, tp, [sp // (SIDE * SIDE), (sp // SIDE) % SIDE, sp % SIDE]


def chip_of(coords):
    return (coords[0] * SIDE + coords[1]) * SIDE + coords[2]


def moved(coords, axis, by):
    return [lax.rem(c + by + SIDE, SIDE) if a == axis else c for a, c in enumerate(coords)]


def gather_kernel(count, *refs):
    packed, swap_in = refs[0], refs[1 : 1 + count]
    whole, swap_out = refs[1 + count], refs[2 + count : 2 + 2 * count]
    own_sem, send, recv, swap_send, swap_recv = refs[2 + 2 * count :]
    sp, tp, me = place()
    own = pltpu.make_async_copy(packed, whole.at[me[0], me[1], me[2]], own_sem)
    own.start()
    barrier = pltpu.get_barrier_semaphore()
    for axis in range(3):
        for by in (1, -1):
            pl.semaphore_signal(
                barrier, inc=1, device_id=(chip_of(moved(me, axis, by)), tp), device_id_type=MESH
            )
    pl.semaphore_signal(barrier, inc=1, device_id=(sp, 1 - tp), device_id_type=MESH)
    pl.semaphore_wait(barrier, 7)

    def part(coords, done, first, tiles):
        index = [slice(None) if a in done else coords[a] for a in range(3)]
        return whole.at[index[0], index[1], index[2], pl.ds(first, tiles)]

    def copy(piece, sems, axis, by):
        return pltpu.make_async_remote_copy(
            src_ref=piece,
            dst_ref=piece,
            send_sem=send.at[sems],
            recv_sem=recv.at[sems],
            device_id=(chip_of(moved(me, axis, by)), tp),
            device_id_type=MESH,
        )

    def halves(colour):
        first, tiles = COLOURS[colour]
        low = tiles // 2
        return ((first, low), (first + low, tiles - low))

    own.wait()
    swaps = [
        pltpu.make_async_remote_copy(
            src_ref=swap_in[k],
            dst_ref=swap_out[k],
            send_sem=swap_send.at[k],
            recv_sem=swap_recv.at[k],
            device_id=(sp, 1 - tp),
            device_id_type=MESH,
        )
        for k in range(count)
    ]
    for phase in range(3):
        sent = []
        for colour in range(3):
            axis, done = ORDERS[colour][phase], ORDERS[colour][:phase]
            low, high = halves(colour)
            for by, pair in ((1, (low, high)), (-1, (high, low))):
                for kind in range(2):
                    go = copy(part(me, done, *pair[kind]), (colour, phase, kind, (by + 1) // 2), axis, by)
                    go.start()
                    sent.append(go)
        if phase == 0:
            for s in swaps:
                s.start()
        for colour in range(3):
            axis, done = ORDERS[colour][phase], ORDERS[colour][:phase]
            low, high = halves(colour)
            for by, piece in ((1, low), (-1, high)):
                came = part(moved(me, axis, -by), done, *piece)
                copy(came, (colour, phase, 0, (by + 1) // 2), axis, by).wait_recv()
                go = copy(came, (colour, phase, 2, (by + 1) // 2), axis, by)
                go.start()
                sent.append(go)
        for colour in range(3):
            axis, done = ORDERS[colour][phase], ORDERS[colour][:phase]
            low, high = halves(colour)
            for by, near, far in ((1, high, low), (-1, low, high)):
                copy(
                    part(moved(me, axis, -by), done, *near), (colour, phase, 1, (by + 1) // 2), axis, by
                ).wait_recv()
                copy(
                    part(moved(me, axis, -2 * by), done, *far), (colour, phase, 2, (by + 1) // 2), axis, by
                ).wait_recv()
        for go in sent:
            go.wait_send()
    for s in swaps:
        s.wait()


def gather(packed, *swapped):
    count = len(swapped)
    return pl.pallas_call(
        functools.partial(gather_kernel, count),
        out_shape=(
            jax.ShapeDtypeStruct((SIDE, SIDE, SIDE, *packed.shape), packed.dtype),
            *(jax.ShapeDtypeStruct(a.shape, a.dtype) for a in swapped),
        ),
        in_specs=[ANY] * (1 + count),
        out_specs=(VMEM, *([ANY] * count)),
        scratch_shapes=[
            pltpu.SemaphoreType.DMA,
            pltpu.SemaphoreType.DMA((3, 3, 3, 2)),
            pltpu.SemaphoreType.DMA((3, 3, 3, 2)),
            pltpu.SemaphoreType.DMA((count,)),
            pltpu.SemaphoreType.DMA((count,)),
        ],
        compiler_params=pltpu.CompilerParams(collective_id=0, has_side_effects=True),
        name="gather",
    )(packed, *swapped)


def attention_kernel(whole, q_own, q_other, up_own, up_other, out, q_all, keys, values, total, top, mass):
    heads = 8
    queries = q_own.shape[1] // (heads // 2)
    sp, tp = lax.axis_index("sp"), lax.axis_index("tp")
    rows = whole.shape[1] * 128
    top[...] = jnp.full(top.shape, NEG_LARGE, jnp.float32)
    mass[...] = jnp.zeros(mass.shape, jnp.float32)
    total[...] = jnp.zeros(total.shape, jnp.float32)
    last = sp // SIDE

    def group(g, masked):
        for b in range(SIDE):
            block = slice(b * 128, (b + 1) * 128)
            left = whole[g, b, pl.ds(0, 8)].reshape(128, 128)
            right = whole[g, b, pl.ds(8, 8)].reshape(128, 128)
            turned = whole[g, b, pl.ds(16, 4)].reshape(64, 128)
            keys[block, 0:128] = left
            keys[block, 128:256] = right
            keys[b * 128 : b * 128 + 64, 256:384] = turned
            keys[b * 128 + 64 : b * 128 + 128, 256:384] = pltpu.roll(turned, 64, 1)
        values[...] = keys[:, 0:256].T
        if masked:
            row = lax.broadcasted_iota(jnp.int32, (rows, queries), 0)
            column = lax.broadcasted_iota(jnp.int32, (rows, queries), 1)
            key_segment = (g * SIDE + row // 128) * 4 + tp * 2 + (row % 128) // SEGMENT
            allowed = key_segment <= sp * 4 + column // SEGMENT
        for h in range(heads):
            q = (q_own, q_other)[h // 4]
            at = slice((h % 4) * queries, (h % 4 + 1) * queries)
            scores = jnp.dot(keys[...], q[:, at], preferred_element_type=jnp.float32)
            if masked:
                scores = jnp.where(allowed, scores, NEG_LARGE)
            old = top[h : h + 1, :]
            new = jnp.maximum(old, jnp.max(scores, axis=0, keepdims=True))
            weights = jnp.exp2(scores - new)
            shrink = jnp.exp2(old - new)
            top[h : h + 1, :] = new
            mass[h : h + 1, :] = mass[h : h + 1, :] * shrink + jnp.sum(weights, axis=0, keepdims=True)
            product = jnp.dot(values[...], weights.astype(jnp.bfloat16), preferred_element_type=jnp.float32)
            total[h] = total[h] * shrink + product

    group(last, True)
    lax.fori_loop(0, last, lambda g, c: (group(g, False), c)[1], 0)
    for b in range(2):
        first = jnp.where(b == 0, tp, 1 - tp) * 512
        up = (up_own, up_other)[b]
        for h in range(4):
            latent_out = total[b * 4 + h].astype(jnp.bfloat16)
            here = lax.dot_general(
                latent_out, up[:, h * 128 : (h + 1) * 128], (((0,), (0,)), ((), ())), preferred_element_type=jnp.float32
            )
            out[:, pl.ds(pl.multiple_of(first + h * 128, 128), 128)] = here
    stats = jnp.concatenate([top[...], mass[...], jnp.zeros((112, queries), jnp.float32)], axis=0)
    out[:, 1024:1152] = stats.T


def attend(whole, q_own, q_other, up_own, up_other):
    queries = q_own.shape[1] // 4
    return pl.pallas_call(
        attention_kernel,
        out_shape=jax.ShapeDtypeStruct((queries, 1152), jnp.float32),
        in_specs=[VMEM] * 5,
        out_specs=VMEM,
        scratch_shapes=[
            pltpu.VMEM((8, 128), jnp.float32),
            pltpu.VMEM((512, 384), jnp.bfloat16),
            pltpu.VMEM((256, 512), jnp.bfloat16),
            pltpu.VMEM((8, 256, queries), jnp.float32),
            pltpu.VMEM((8, queries), jnp.float32),
            pltpu.VMEM((8, queries), jnp.float32),
        ],
        compiler_params=pltpu.CompilerParams(vmem_limit_bytes=56 * 1024 * 1024),
        name="attend",
    )(whole, q_own, q_other, up_own, up_other)


def exchange_kernel(outgoing, arrived, own_sem, send, recv):
    sp, tp, _ = place()
    barrier = pltpu.get_barrier_semaphore()

    def greet(k, carry):
        pl.semaphore_signal(barrier, inc=1, device_id=(lax.rem(sp + k, CHIPS), tp), device_id_type=MESH)
        return carry

    lax.fori_loop(1, CHIPS, greet, 0)
    own = pltpu.make_async_copy(outgoing.at[sp], arrived.at[sp], own_sem)
    own.start()
    pl.semaphore_wait(barrier, CHIPS - 1)

    def to(k):
        dz, dy, dx = k // 16, (k // 4) % 4, k % 4
        z, y, x = sp // 16, (sp // 4) % 4, sp % 4
        return (lax.rem(z + dz, 4) * 4 + lax.rem(y + dy, 4)) * 4 + lax.rem(x + dx, 4)

    def start(k, carry):
        peer = to(k)
        pltpu.make_async_remote_copy(
            src_ref=outgoing.at[peer],
            dst_ref=arrived.at[sp],
            send_sem=send,
            recv_sem=recv,
            device_id=(peer, tp),
            device_id_type=MESH,
        ).start()
        return carry

    lax.fori_loop(1, CHIPS, start, 0)
    own.wait()
    most = pl.ds(0, CHIPS - 1)
    every = pltpu.make_async_remote_copy(
        src_ref=outgoing.at[most],
        dst_ref=arrived.at[most],
        send_sem=send,
        recv_sem=recv,
        device_id=(sp, 1 - tp),
        device_id_type=MESH,
    )
    every.wait_send()
    every.wait_recv()


def exchange(outgoing, number):
    return pl.pallas_call(
        exchange_kernel,
        out_shape=jax.ShapeDtypeStruct(outgoing.shape, outgoing.dtype),
        in_specs=[ANY],
        out_specs=ANY,
        scratch_shapes=[pltpu.SemaphoreType.DMA, pltpu.SemaphoreType.DMA, pltpu.SemaphoreType.DMA],
        compiler_params=pltpu.CompilerParams(collective_id=number, has_side_effects=True),
        name=f"exchange{number}",
    )(outgoing)


def local(
    residual,
    query_nope,
    query_rope,
    latent,
    key_rope,
    key_up,
    value_up,
    out_proj,
    norm_gain,
    routes,
    route_weight,
    w_gate,
    w_up,
    w_down,
):
    tp = lax.axis_index("tp")
    sp = lax.axis_index("sp")
    row_count = residual.shape[0]
    queries = query_nope.shape[0]
    heads_here = query_nope.shape[1] // QK_NOPE
    scale = (QK_NOPE + QK_ROPE) ** (-0.5) * LOG2_E
    query_first = sp * queries
    query_pos = query_first + jnp.arange(queries, dtype=jnp.int32)
    query_rot = rotary(query_rope.astype(jnp.float32).reshape(queries, heads_here, QK_ROPE), query_pos)
    rot_side = jnp.transpose(query_rot * scale, (2, 1, 0)).astype(jnp.bfloat16).reshape(QK_ROPE, -1)
    latent_side = jnp.einsum(
        "lhd,qhd->lhq",
        key_up.reshape(-1, heads_here, QK_NOPE),
        query_nope.reshape(queries, heads_here, QK_NOPE),
        preferred_element_type=jnp.float32,
    )
    latent_side = (latent_side * scale).astype(jnp.bfloat16).reshape(latent_side.shape[0], -1)
    q_own = jnp.concatenate([latent_side, rot_side, jnp.zeros_like(rot_side)], axis=0)
    key_pos = query_first + tp * row_count + jnp.arange(row_count, dtype=jnp.int32)
    key_rot = rotary(key_rope.astype(jnp.float32), key_pos).astype(jnp.bfloat16)
    packed = jnp.concatenate(
        [
            latent[:, :128].reshape(8, 16, 128),
            latent[:, 128:].reshape(8, 16, 128),
            jnp.concatenate([key_rot[:64], key_rot[64:]], axis=1).reshape(4, 16, 128),
        ],
        axis=0,
    )
    gate_own, up_own, down_own = w_gate[0], w_up[0], w_down[0]
    whole, q_other, value_other, gate_other, up_other, down_other = gather(
        packed, q_own, value_up, gate_own, up_own, down_own
    )
    partial = attend(whole.reshape(SIDE * SIDE, SIDE, TILES, 16, 128), q_own, q_other, value_up, value_other)
    both = lax.all_to_all(
        partial.reshape(2, row_count, 1152), "tp", split_axis=0, concat_axis=0, tiled=True
    )
    order = jnp.arange(2, dtype=jnp.int32)[:, None, None]

    def by_head(stats):
        return jnp.where(order == 0, stats, jnp.concatenate([stats[..., 4:], stats[..., :4]], axis=-1))

    top, mass = by_head(both[:, :, 1024:1032]), by_head(both[:, :, 1032:1040])
    factor = jnp.exp2(top - jnp.max(top, axis=0, keepdims=True))
    factor = factor / jnp.sum(factor * mass, axis=0, keepdims=True)
    weighted = both[:, :, :1024].reshape(2, row_count, 8, V_DIM)
    attn_out = jnp.sum(weighted * factor[..., None], axis=0).astype(jnp.bfloat16).reshape(row_count, 1024)
    projected = jnp.dot(attn_out, out_proj, preferred_element_type=jnp.float32)
    hidden_wide = residual.astype(jnp.float32) + projected
    hidden = hidden_wide.astype(jnp.bfloat16)
    hidden_wide = hidden.astype(jnp.float32)
    normed = hidden_wide * lax.rsqrt(
        jnp.mean(hidden_wide * hidden_wide, axis=-1, keepdims=True) + EPSILON
    )
    normed = (normed * norm_gain[None, :]).astype(jnp.bfloat16)
    expert_count = CHIPS
    capacity = 8
    top_count = routes.shape[1]
    width = normed.shape[1]
    flat_expert = routes.reshape(-1)
    onehot = (flat_expert[:, None] == jnp.arange(expert_count, dtype=jnp.int32)[None, :]).astype(
        jnp.int32
    )
    slot_rank = jnp.sum(jnp.cumsum(onehot, axis=0) * onehot, axis=1) - 1
    slot_index = flat_expert * capacity + slot_rank
    outgoing = (
        jnp.zeros((expert_count * capacity, width), jnp.bfloat16)
        .at[slot_index]
        .set(jnp.repeat(normed, top_count, axis=0))
    )
    rows = exchange(outgoing.reshape(expert_count, capacity, width), 1).reshape(-1, width)

    def half(gate, up, down):
        gate_part = jnp.dot(rows, gate, preferred_element_type=jnp.float32)
        up_part = jnp.dot(rows, up, preferred_element_type=jnp.float32)
        activated = (jax.nn.silu(gate_part) * up_part).astype(jnp.bfloat16)
        return jnp.dot(activated, down, preferred_element_type=jnp.float32)

    expert_out = (half(gate_own, up_own, down_own) + half(gate_other, up_other, down_other)).astype(jnp.bfloat16)
    back_rows = exchange(expert_out.reshape(expert_count, capacity, width), 2)
    picked = back_rows.reshape(expert_count * capacity, width)[slot_index]
    combined = jnp.sum(
        picked.astype(jnp.float32).reshape(row_count, top_count, width) * route_weight[:, :, None],
        axis=1,
    )
    return (hidden_wide + combined).astype(jnp.bfloat16)


def solution(mesh):
    return jax.shard_map(
        local,
        mesh=mesh,
        in_specs=(
            P(("sp", "tp"), None),
            P("sp", "tp"),
            P("sp", "tp"),
            P(("sp", "tp"), None),
            P(("sp", "tp"), None),
            P(None, "tp"),
            P(None, "tp"),
            P(),
            P(),
            P(("sp", "tp"), None),
            P(("sp", "tp"), None),
            P("sp", None, "tp"),
            P("sp", None, "tp"),
            P("sp", "tp", None),
        ),
        out_specs=P(("sp", "tp"), None),
        check_vma=False,
    )
```

time: 447 us -> 249 us (0.56)
  Pallas kernels: 0 us -> 190 us
  matrix products: 157 us -> 21 us
  waiting for transfers between devices: 113 us -> 1.48 us
  blocking collectives: 58.2 us -> 0 us
  other arithmetic: 43.7 us -> 8.31 us
  local copies, waits for them, and re-layouts: 53.1 us -> 18.2 us
  between operations: 13.7 us -> 0.3 us
    pallas_call x0 -> x4, Pallas kernels: none -> 190 us  [the longest x2 145 us: exchange(): pl.pallas_call(exchange_kernel, out_shape=jax.ShapeDtypeStruct(outgoing.s...]
    dot_general x43 -> x6, matrix products: 157 us -> 21 us  [the longest x2 12.6 us: half(): return jnp.dot(activated, down, preferred_element_type=jnp.float32)]
    all_gather x1 -> x0, waiting for transfers between devices: 84 us -> none  [side_by_side(): lax.all_gather(both, axis, axis=dim, tiled=True)]
    all_to_all x4 -> x0, blocking collectives: 58.2 us -> none  [the longest x1 37.3 us: local(): lax.all_to_all(outgoing.reshape(expert_count, capacity, width), 'sp', spl...]
    all_to_all x1, waiting for transfers between devices: 29 us -> 1.48 us  [local(): lax.all_to_all(partial.reshape(2, row_count, 1152), 'tp', split_axis=0, c...]
    slice x4 -> x3, local copies, waits for them, and re-layouts: 21.6 us -> 0.98 us  [the longest x1 0.79 us: local(): latent[:, :128].reshape(8, 16, 128)]
    reduce_sum x9 -> x2, other arithmetic: 15.6 us -> 0.16 us  [the longest x1 0.08 us: local(): jnp.sum(weighted * factor[..., None], axis=0).astype(jnp.bfloat16)]
    add x9 -> x0, other arithmetic: 9.57 us -> none  [the longest x8 9.57 us: one_block(): new_sum = old_sum * shrink + jnp.sum(weights, axis=-1)]
  transfers between devices with their start and end apart: 2 -> 1, of which waited for: 2 -> 1; matrix products, arithmetic and copies ran while one was open for 1% -> 0% of each run, Pallas kernels for 0% -> 0%
where the time goes in v1:
time: 249 us; the launch traced here: 247 us
  Pallas kernels  190 us (76%)
  matrix products  21 us (8%)
  local copies, waits for them, and re-layouts  18.2 us (7%)
  other arithmetic  8.31 us (3%)
  starting transfers between devices  7.96 us (3%)
    pallas_call x2, Pallas kernels, exchange(): pl.pallas_call(exchange_kernel, out_shape=jax.ShapeDtypeStruct(outgoing.s...  145 us
    pallas_call x1, Pallas kernels, gather(): pl.pallas_call(functools.partial(gather_kernel, count), out_shape=(jax.Sh...  35.6 us
    dot_general x2, matrix products, half(): return jnp.dot(activated, down, preferred_element_type=jnp.float32)  12.6 us
    pallas_call x1, Pallas kernels, attend(): pl.pallas_call(attention_kernel, out_shape=jax.ShapeDtypeStruct((queries,...  9.47 us
    all_to_all x1, starting transfers between devices, local(): lax.all_to_all(partial.reshape(2, row_count, 1152), 'tp', split_axis=0, c...  7.96 us
    gather x1, local copies, waits for them, and re-layouts, local(): picked = back_rows.reshape(expert_count * capacity, width)[slot_index]  5.21 us
    dot_general x2, matrix products, half(): gate_part = jnp.dot(rows, gate, preferred_element_type=jnp.float32)  5.06 us
  transfers between devices with their start and end apart: 1, of which 1 were waited for; matrix products, arithmetic and copies ran while one was open for 0% of the time, Pallas kernels for 0%

profile of v1, /device:TPU:1, one launch (start us, length us, event | category | flops | bytes accessed | tf_op | source)
XLA Modules:
  0.0 247.2 jit_solution(7431468660406466170)
XLA Ops:
  0.0 0.0 copy-start
  0.1 0.8 convert_element_type.72
  0.8 0.1 fusion.60
  1.0 0.1 fusion.54
  1.1 0.1 copy.45
  1.2 0.8 fusion.74
  1.9 0.2 multiply_cosine_fusion
  2.1 1.0 copy.49
  3.3 0.3 fusion.11
  3.6 0.2 copy.57
  3.8 0.1 pad.6.clone
  3.9 0.6 pad_maximum_fusion.refs_0_
  4.6 1.1 maximum_maximum_fusion.refs_1_.q_own
  5.6 35.6 %gather.7 = (bf16[4,4,4,20,16,128]{5,4,3,2,1,0:T(8,128)(2,1)}, bf16[384,1024]{1,0:T(8,128)(2,1)}, bf16[256,512]{1,0:T(8,128)(2,1)}, bf16[2048,256]{1,0:T(8,128)(...) custom-call(bf16[20,16,128]{2,1,0:T(8,128)(2,1)} %pad_maximum_fusion.refs_0_, ...), custom_call_target="tpu_custom_call" | custom-call | tf_op jit(solution)/shard_map/gather/pallas_call | solution.py:144
  41.2 9.5 %attend.1 = f32[256,1152]{1,0:T(8,128)} custom-call(bf16[16,4,20,16,128]{4,3,2,1,0:T(8,128)(2,1)} %bitcast.89, bf16[384,1024]{1,0:T(8,128)(2,1)} %maximum_maximum_fusion.refs_1_.q_own, bf16[384,1024]{1,0:T(8,128)(2,1)} %get-tuple-element.12.q_other, bf16[256,512]{1,0:T(8,128)(2,1)} %up_own.1, bf16[256,512]{1,0:T(8,128)(2,1)} %get-tuple-element.13.up_other), custom_call_target="tpu_custom_call" | custom-call | tf_op jit(solution)/shard_map/attend/pallas_call | solution.py:222
  50.7 2.7 %copy.51 = f32[2,128,1152]{1,2,0:T(8,128)} copy(f32[2,128,1152]{2,1,0:T(8,128)} %bitcast.90) | data formatting | bytes 2359296 | tf_op jit(solution)/shard_map/reshape | solution.py:347
  53.4 8.0 %all-to-all-start = ((f32[2,128,1152]{1,2,0:T(8,128)}), f32[2,128,1152]{1,2,0:T(8,128)S(1)}, u32[]{:S(2)}, u32[]{:S(2)}) async-start(f32[2,128,1152]{1,2,0:T(8,128)} %copy.51), calls=%async_computation | async-start | bytes 2359296 | tf_op jit(solution)/shard_map/all_to_all | solution.py:346
  61.3 0.1 copy.53
  61.4 0.1 eq.41
  61.6 0.1 eq.37
  61.7 1.5 all-to-all-done
  63.2 0.1 fusion.72
  63.3 0.1 fusion.64
  63.4 0.1 fusion.27
  63.5 0.0 copy-start.4
  63.5 3.0 %multiply_reduce_fusion.1 = (f32[128]{0:T(128)S(1)}, f32[128,2048]{1,0:T(8,128)S(1)}) fusion(bf16[128,1024]{0,1:T(8,128)(2,1)S(1)} %fusion.27, bf16[1024,2048]{1,0:T(8,128)(2,1)} %param.21, bf16[128,2048]{1,0:T(8,128)(2,1)S(1)} %copy-done.2), kind=kOutput, calls=%fused_computation.27 | convolution fusion | flops 538443648 | bytes 6029824 | tf_op jit(solution)/shard_map/dot_general | solution.py:359
  66.5 0.2 multiply_convert_fusion
  66.7 0.6 broadcast_in_dim.22
  67.3 0.4 reshape.221
  67.8 0.6 reduce-window.6
  68.4 0.2 slice_reduce_fusion
  68.6 0.1 fusion.52
  68.8 0.1 copy.52
  68.9 0.1 mul.196
  69.0 3.7 %scatter_custom_fusion = bf16[512,2048]{1,0:T(8,128)(2,1)} fusion(s32[256]{0:T(256)S(1)} %bitcast.101, bf16[256,2048]{1,0:T(8,128)(2,1)S(1)} %reshape.221, bf16[]{:T(256)} %constant.25.clone.1), kind=kCustom, calls=%fused_computation.28 | custom fusion | bytes 2097154 | tf_op jit(solution)/shard_map/scatter | solution.py:380
  72.8 107.5 %exchange1.1 = bf16[64,8,2048]{2,1,0:T(8,128)(2,1)} custom-call(bf16[64,8,2048]{2,1,0:T(8,128)(2,1)} %bitcast.88), custom_call_target="tpu_custom_call" | custom-call | tf_op jit(solution)/shard_map/exchange1/pallas_call | solution.py:286
  180.3 3.5 %fusion.9 = f32[512,256]{1,0:T(8,128)} fusion(bf16[64,8,2048]{2,1,0:T(8,128)(2,1)} %exchange1.1, bf16[1,2048,256]{2,1,0:T(8,128)(2,1)} %param.25), kind=kOutput, calls=%fused_computation.13 | convolution fusion | flops 536870912 | bytes 3670016 | tf_op jit(solution)/shard_map/dot_general | solution.py:385
  183.8 0.0 copy-done.1
  183.8 1.5 fusion.5
  185.4 5.9 %fusion.25 = f32[512,2048]{1,0:T(8,128)} fusion(bf16[64,8,2048]{2,1,0:T(8,128)(2,1)S(1)} %copy-done.1, f32[512,256]{1,0:T(8,128)} %fusion.9, bf16[1,256,2048]{2,1,0:T(8,128)(2,1)} %param.27, bf16[1,2048,256]{2,1,0:T(8,128)(2,1)} %param.26), kind=kOutput, calls=%fused_computation.22 | convolution fusion | flops 1074528256 | bytes 8912896 | tf_op jit(solution)/shard_map/dot_general | solution.py:388
  191.3 6.6 %fusion.outgoing = bf16[64,8,2048]{2,1,0:T(8,128)(2,1)} fusion(f32[512,2048]{1,0:T(8,128)} %fusion.25, bf16[256,2048]{1,0:T(8,128)(2,1)} %get-tuple-element.16, bf16[2048,256]{1,0:T(8,128)(2,1)} %get-tuple-element.15, bf16[64,8,2048]{2,1,0:T(8,128)(2,1)S(1)} %copy-done.1, f32[512,256]{1,0:T(8,128)} %fusion.5), kind=kOutput, calls=%fused_computation.3 | convolution fusion | flops 1076625408 | bytes 11010048 | tf_op jit(solution)/shard_map/dot_general | solution.py:388
  198.0 37.4 %exchange2.1 = bf16[64,8,2048]{2,1,0:T(8,128)(2,1)} custom-call(bf16[64,8,2048]{2,1,0:T(8,128)(2,1)} %fusion.outgoing), custom_call_target="tpu_custom_call" | custom-call | tf_op jit(solution)/shard_map/exchange2/pallas_call | solution.py:286
  235.3 5.2 %gather_fusion = bf16[256,2048]{1,0:T(8,128)(2,1)} fusion(bf16[512,2048]{1,0:T(8,128)(2,1)} %bitcast.87, s32[1024]{0:T(1024)S(1)} %pad_clamp_fusion), kind=kCustom, calls=%fused_computation | custom fusion | bytes 2098176 | tf_op jit(solution)/shard_map/gather | solution.py:392
  240.6 2.4 reshape.208
  242.9 0.0 copy-done.6
  243.0 0.1 copy.56
  243.1 3.2 %multiply_reduce_fusion = f32[128,2048]{1,0:T(8,128)S(1)} fusion(f32[128,2,2048]{2,1,0:T(2,128)S(1)} %reshape.208, f32[128,2]{1,0:T(8,128)S(1)} %copy.56), kind=kLoop, calls=%fused_computation.15 | loop fusion | flops 786432 | bytes 3146752 | tf_op jit(solution)/shard_map/reduce_sum | solution.py:393
  246.2 0.9 add_convert_fusion.1
  (32 shorter events, 0.2 us)
Async XLA Ops:
  0.0 3.3 %copy-start = (bf16[256,512]{1,0:T(8,128)(2,1)S(1)}, bf16[256,512]{1,0:T(8,128)(2,1)}, u32[]{:S(2)}) copy-start(bf16[256,512]{1,0:T(8,128)(2,1)} %param.19) | copy-start | bytes 786436
  0.0 3.3 %copy-start.3 = (bf16[256,512]{1,0:T(8,128)(2,1)S(1)}, bf16[256,512]{1,0:T(8,128)(2,1)}, u32[]{:S(2)}) copy-start(bf16[256,512]{1,0:T(8,128)(2,1)} %param.15) | copy-start | bytes 786436
  50.7 10.6 %copy-start.5 = (s32[128,2]{0,1:T(2,128)S(1)}, s32[128,2]{0,1:T(2,128)}, u32[]{:S(2)}) copy-start(s32[128,2]{0,1:T(2,128)} %param.23) | copy-start | bytes 3076
  53.4 10.1 %copy-start.2 = (bf16[128,2048]{1,0:T(8,128)(2,1)S(1)}, bf16[128,2048]{1,0:T(8,128)(2,1)}, u32[]{:S(2)}) copy-start(bf16[128,2048]{1,0:T(8,128)(2,1)} %param.14) | copy-start | bytes 1572868
  53.4 9.9 %all-to-all-start = ((f32[2,128,1152]{1,2,0:T(8,128)}), f32[2,128,1152]{1,2,0:T(8,128)S(1)}, u32[]{:S(2)}, u32[]{:S(2)}) async-start(f32[2,128,1152]{1,2,0:T(8,128)} %copy.51), calls=%async_computation | async-start | bytes 2359296 | tf_op jit(solution)/shard_map/all_to_all | solution.py:346
  63.5 3.0 %copy-start.4 = (f32[2048]{0:T(1024)S(1)}, f32[2048]{0:T(1024)}, u32[]{:S(2)}) copy-start(f32[2048]{0:T(1024)} %param.22) | copy-start | bytes 24580
  180.3 3.5 %copy-start.1 = (bf16[64,8,2048]{2,1,0:T(8,128)(2,1)S(1)}, bf16[64,8,2048]{2,1,0:T(8,128)(2,1)}, u32[]{:S(2)}) copy-start(bf16[64,8,2048]{2,1,0:T(8,128)(2,1)} %exchange1.1) | copy-start | bytes 6291460
  180.3 3.5 %copy-start.7 = (bf16[2048,256]{1,0:T(8,128)(2,1)S(1)}, bf16[2048,256]{1,0:T(8,128)(2,1)}, u32[]{:S(2)}) copy-start(bf16[2048,256]{1,0:T(8,128)(2,1)} %get-tuple-element.14) | copy-start | bytes 3145732
  240.6 2.4 copy-start.6
